TPU v7x, 32 devices: a whole 2x2x4 slice. The times are simulated.
32 devices in a mesh: sp: 8 (over z, x), tp: 4 (over y, core).
Axes of the slice: x: 2, y: 2, z: 4, core: 2. Of those that a mesh axis runs over, the one named last changes fastest.
Arguments:
- layer_grad: bfloat16 [2048, 2048], P('sp', 'tp'), may hold values from -6 to 6
- routes: int32 [2048, 2], P('sp'), may hold values from 0 to 7, all different within a row; in each aligned block of 256 rows (0 to 255, 256 to 511, ...) at most 96 rows name the same one
- route_weights: float32 [2048, 2], P('sp'), may hold values from 0.1 to 0.9
- expert_in: bfloat16 [8, 768, 2048], P('sp', None, 'tp'), may hold values from -50 to 50
- w_gate: bfloat16 [8, 2048, 2048], P('sp', None, 'tp'), may hold values from -0.125 to 0.125
- w_up: bfloat16 [8, 2048, 2048], P('sp', None, 'tp'), may hold values from -0.125 to 0.125
- w_down: bfloat16 [8, 2048, 2048], P('sp', 'tp'), may hold values from -0.125 to 0.125
- conv_in: bfloat16 [2048, 512], P('sp', 'tp'), may hold values from -6 to 6
- c_gate: bfloat16 [2048, 512], P('sp', 'tp'), may hold values from -6 to 6
- b_gate: bfloat16 [2048, 512], P('sp', 'tp'), may hold values from -1.5 to 1.5
- conv_out: bfloat16 [2048, 512], P('sp', 'tp'), may hold values from -1.5 to 1.5
- taps: bfloat16 [3, 512], P(None, 'tp'), may hold values from -3.5 to 3.5
- w_out: bfloat16 [512, 2048], P('tp'), may hold values from -0.25 to 0.25
Outputs:
- grad_w_gate: bfloat16 [8, 2048, 2048], P('sp', None, 'tp')
- grad_w_up: bfloat16 [8, 2048, 2048], P('sp', None, 'tp')
- grad_w_down: bfloat16 [8, 2048, 2048], P('sp', 'tp')
- grad_routed: bfloat16 [2048, 2048], P('sp', 'tp')
- grad_out_proj: float32 [512, 2048], P('tp', 'sp')
- grad_conv_in: bfloat16 [2048, 512], P('sp', 'tp')
- grad_c_gate: bfloat16 [2048, 512], P('sp', 'tp')
- grad_b_gate: bfloat16 [2048, 512], P('sp', 'tp')
Inputs may be any that keep to these rules, and one draw needn't show every extreme that they name: `routes`: each token names 2 different experts. Among the tokens of one block of 256, no expert is named more than 96 times, a bound that some block reaches.
All inputs are finite; a program needn't handle non-finite values.
Results may differ from a plain program's by a relative error of at most 0.019.
Values may be sent and summed in bfloat16 or wider, within the bound.
No kernel may reach another device: no remote copies, remote signals or barrier semaphores. Data moves between devices by JAX's collectives and lax.ppermute only.
A program may use at most 64 MiB of HBM per device.

v0:
```python
import jax
import jax.numpy as jnp
from jax import lax
from jax.sharding import PartitionSpec as P

clamp_limit = 7.0
swish_alpha = 1.702


def passed_along(value, axis, steps):
    count = lax.axis_size(axis)
    leading, last = (max(0, -steps), min(count, count - steps))
    return lax.ppermute(value, axis, [(source, source + steps) for source in range(leading, last)])


def per_device(
    layer_grad,
    routes,
    route_weights,
    expert_in,
    w_gate,
    w_up,
    w_down,
    conv_in,
    c_gate,
    b_gate,
    conv_out,
    taps,
    w_out,
):
    sp_devices = lax.axis_size("sp")
    tok_rows = layer_grad.shape[0]
    top_count = routes.shape[1]
    capacity = expert_in.shape[1] // sp_devices
    full_grad = lax.all_gather(layer_grad, "tp", axis=1, tiled=True)
    flat_routes = routes.reshape(-1)
    onehot = (flat_routes[:, None] == jnp.arange(sp_devices, dtype=jnp.int32)[None, :]).astype(
        jnp.int32
    )
    slot_rank = jnp.sum((jnp.cumsum(onehot, axis=0) - 1) * onehot, axis=1)
    slot_index = flat_routes * capacity + slot_rank
    weights = route_weights[:, :, None]
    scaled = (weights * layer_grad[:, None, :].astype(jnp.float32)).astype(jnp.bfloat16)
    scaled = scaled.reshape(tok_rows * top_count, -1)
    buffer = (
        jnp.zeros((sp_devices * capacity, scaled.shape[1]), jnp.bfloat16).at[slot_index].set(scaled)
    )
    arrived = lax.all_to_all(
        buffer.reshape(sp_devices, capacity, -1), "sp", split_axis=0, concat_axis=0, tiled=True
    )
    expert_grad, saved_rows = (
        lax.all_gather(arrived.reshape(sp_devices * capacity, -1), "tp", axis=1, tiled=True),
        lax.all_gather(expert_in[0], "tp", axis=1, tiled=True),
    )
    gate_weight = w_gate[0]
    up_weight = w_up[0]
    down_weight = w_down[0]
    gate_pre = jnp.dot(saved_rows, gate_weight, preferred_element_type=jnp.float32)
    up_pre = jnp.dot(saved_rows, up_weight, preferred_element_type=jnp.float32)
    gate_cut = jnp.minimum(gate_pre, clamp_limit)
    up_cut = jnp.clip(up_pre, -clamp_limit, clamp_limit)
    sigmoid_gate = jax.nn.sigmoid(swish_alpha * gate_cut)
    hidden = ((up_cut + 1.0) * gate_cut * sigmoid_gate).astype(jnp.bfloat16)
    act_grad = jnp.einsum("rd,fd->rf", expert_grad, down_weight, preferred_element_type=jnp.float32)
    grad_down = jnp.einsum(
        "rf,rd->fd", hidden, expert_grad, preferred_element_type=jnp.float32
    ).astype(jnp.bfloat16)
    slope = sigmoid_gate + swish_alpha * gate_cut * sigmoid_gate * (1.0 - sigmoid_gate)
    gate_grad = jnp.where(gate_pre < clamp_limit, act_grad * (up_cut + 1.0) * slope, 0.0).astype(
        jnp.bfloat16
    )
    up_grad = jnp.where(
        jnp.abs(up_pre) < clamp_limit, act_grad * gate_cut * sigmoid_gate, 0.0
    ).astype(jnp.bfloat16)
    grad_gate = jnp.einsum(
        "rd,rf->df", saved_rows, gate_grad, preferred_element_type=jnp.float32
    ).astype(jnp.bfloat16)
    grad_up = jnp.einsum(
        "rd,rf->df", saved_rows, up_grad, preferred_element_type=jnp.float32
    ).astype(jnp.bfloat16)
    partial_value = jnp.einsum(
        "rf,df->rd", gate_grad, gate_weight, preferred_element_type=jnp.float32
    )
    partial_value = partial_value + jnp.einsum(
        "rf,df->rd", up_grad, up_weight, preferred_element_type=jnp.float32
    )
    rounded_terms = partial_value.astype(jnp.bfloat16)
    reduced = (
        lax.psum_scatter(rounded_terms, "tp", scatter_dimension=1, tiled=True)
        .astype(jnp.float32)
        .astype(jnp.bfloat16)
    )
    returned = lax.all_to_all(
        reduced.reshape(sp_devices, capacity, -1), "sp", split_axis=0, concat_axis=0, tiled=True
    )
    returned = returned.reshape(sp_devices * capacity, -1)
    picked = returned[slot_index]
    picked = picked.reshape(tok_rows, top_count, -1)
    grad_routed = jnp.sum(picked.astype(jnp.float32), axis=1).astype(jnp.bfloat16)
    mixer_grad = jnp.einsum("td,cd->tc", full_grad, w_out, preferred_element_type=jnp.float32)
    mixed = (b_gate.astype(jnp.float32) * conv_out.astype(jnp.float32)).astype(jnp.bfloat16)
    projected = lax.psum_scatter(
        jnp.einsum("td,tc->dc", full_grad, mixed, preferred_element_type=jnp.float32),
        "sp",
        scatter_dimension=0,
        tiled=True,
    )
    grad_out_proj = projected.T
    out_grad = mixer_grad * b_gate.astype(jnp.float32)
    tap_reach = taps.shape[0] - 1
    following = passed_along(out_grad[:tap_reach], "sp", -1)
    extended = jnp.concatenate([out_grad, following], axis=0)
    tap_values = taps.astype(jnp.float32)
    conv_grad = jnp.zeros_like(out_grad)
    for tap_index in range(tap_reach + 1):
        offset = tap_reach - tap_index
        conv_grad = conv_grad + tap_values[tap_index] * extended[offset : offset + tok_rows]
    grad_conv_in = (conv_grad * c_gate.astype(jnp.float32)).astype(jnp.bfloat16)
    grad_c_gate = (conv_grad * conv_in.astype(jnp.float32)).astype(jnp.bfloat16)
    grad_b_gate = (mixer_grad * conv_out.astype(jnp.float32)).astype(jnp.bfloat16)
    return (
        grad_gate[None],
        grad_up[None],
        grad_down[None],
        grad_routed,
        grad_out_proj,
        grad_conv_in,
        grad_c_gate,
        grad_b_gate,
    )


def solution(mesh):
    in_specs = (
        P("sp", "tp"),
        P("sp", None),
        P("sp", None),
        P("sp", None, "tp"),
        P("sp", None, "tp"),
        P("sp", None, "tp"),
        P("sp", "tp", None),
        P("sp", "tp"),
        P("sp", "tp"),
        P("sp", "tp"),
        P("sp", "tp"),
        P(None, "tp"),
        P("tp", None),
    )
    out_specs = (
        P("sp", None, "tp"),
        P("sp", None, "tp"),
        P("sp", "tp", None),
        P("sp", "tp"),
        P("tp", "sp"),
        P("sp", "tp"),
        P("sp", "tp"),
        P("sp", "tp"),
    )
    return jax.shard_map(
        per_device, mesh=mesh, in_specs=in_specs, out_specs=out_specs, check_vma=False
    )
```

profile of v0, /device:TPU:0, one launch (start us, length us, event | category | flops | bytes accessed | tf_op | source)
XLA Modules:
  0.0 212.0 jit_solution(14027986862488300360)
XLA Ops:
  7.2 0.0 copy-start
  7.2 0.0 all-gather.9.cloned.1.call-start
  7.2 0.7 all-gather.9.cloned.1.call-update
  7.9 0.0 copy-start.11
  7.9 0.0 all-gather.5.cloned.1.call-start
  8.0 0.8 copy.24
  8.8 0.1 eq.29
  8.9 0.1 eq.25
  9.1 0.7 broadcast_multiply_fusion
  9.8 0.1 copy.23
  9.9 0.1 mul.112
  10.1 1.1 reduce-window.6
  11.2 0.2 slice_reduce_fusion
  11.5 2.2 %mul.116 = f32[256,2,512]{2,1,0:T(2,128)} broadcast(bf16[256,512]{1,0:T(8,128)(2,1)} %param.13), dimensions={0,2} | broadcast | bytes 1310720 | tf_op jit(solution)/shard_map/mul | solution.py:43
  13.7 1.9 mul.117
  15.6 0.0 copy-done.11
  15.6 0.1 copy.26
  15.8 0.1 mul.114
  15.9 0.1 fusion.43
  16.0 3.4 %scatter_custom_fusion = bf16[768,512]{1,0:T(8,128)(2,1)} fusion(s32[512]{0:T(512)S(1)} %bitcast.76, f32[512,512]{1,0:T(8,128)S(1)} %mul.117, f32[512]{0:T(512)S(1)} %mul.114, bf16[]{:T(256)} %constant.11.clone.1), kind=kCustom, calls=%fused_computation.36 | custom fusion | flops 524288 | bytes 1837058 | tf_op jit(solution)/shard_map/scatter | solution.py:46
  19.4 27.5 %all_to_all.10 = bf16[8,96,512]{2,1,0:T(8,128)(2,1)} all-to-all(bf16[8,96,512]{2,1,0:T(8,128)(2,1)} %bitcast.73), channel_id=1, replica_groups=mesh['sp'=8,'tp'=4] {'sp'}, dimensions={0} | all-to-all | bytes 1572864 | tf_op jit(solution)/shard_map/all_to_all | solution.py:48
  46.9 0.0 all-gather.5.cloned.1.call-update
  47.0 0.0 all-gather.7.cloned.1.call-start
  47.0 0.7 all-gather.7.cloned.1.call-update
  47.7 0.2 reduce-scatter.3.cloned.1.call-start
  47.9 0.0 all-gather.9.cloned.1.call-done
  47.9 0.0 copy-start.1
  48.0 5.6 %fusion.4 = f32[768,512]{1,0:T(8,128)} fusion(bf16[1,768,2048]{2,1,0:T(8,128)(2,1)} %all-gather.9.cloned.1.call-done, bf16[1,2048,512]{2,1,0:T(8,128)(2,1)} %param.18), kind=kOutput, calls=%fused_computation.7 | convolution fusion | flops 1610612736 | bytes 6815744 | tf_op jit(solution)/shard_map/dot_general | solution.py:59
  53.6 0.0 copy-done
  53.6 0.0 copy-done.1
  53.6 3.0 %fusion.6 = f32[768,512]{1,0:T(8,128)} fusion(bf16[1,768,2048]{2,1,0:T(8,128)(2,1)S(1)} %copy-done.1, bf16[1,2048,512]{2,1,0:T(8,128)(2,1)S(1)} %copy-done), kind=kOutput, calls=%fused_computation.9 | convolution fusion | flops 1610612736 | bytes 6815744 | tf_op jit(solution)/shard_map/dot_general | solution.py:58
  56.6 18.1 %all-gather.5.cloned.1.call-done = bf16[768,2048]{1,0:T(8,128)(2,1)} async-done(((bf16[768,512]{1,0:T(8,128)(2,1)}), bf16[768,2048]{1,0:T(8,128)(2,1)}) %all-gather.5.cloned.1.call-update) | async-done | bytes 3145744 | tf_op jit(solution)/shard_map/all_gather | solution.py:52
  74.7 6.1 %select_convert_fusion = (bf16[768,512]{1,0:T(8,128)(2,1)S(1)}, bf16[768,512]{1,0:T(8,128)(2,1)S(1)}) fusion(f32[768,512]{1,0:T(8,128)} %fusion.4, f32[768,512]{1,0:T(8,128)} %fusion.6, bf16[768,2048]{1,0:T(8,128)(2,1)} %all-gather.5.cloned.1.call-done, bf16[1,512,2048]{2,1,0:T(8,128)(2,1)} %param.19), kind=kOutput, calls=%fused_computation.26 | convolution fusion | flops 1619263488 | bytes 9961472 | tf_op jit(solution)/shard_map/rd,fd->rf/dot_general | solution.py:64
  80.8 0.0 copy-start.4
  80.8 0.0 copy-start.3
  80.8 0.0 copy-start.5
  80.8 1.8 fusion.25
  82.7 0.0 copy-done.4
  82.7 0.4 copy-done.5
  83.0 3.5 %add_convert_fusion = bf16[768,2048]{1,0:T(8,128)(2,1)} fusion(f32[768,2048]{1,0:T(8,128)S(1)} %fusion.25, bf16[768,512]{1,0:T(8,128)(2,1)S(1)} %get-tuple-element.26, bf16[1,2048,512]{2,1,0:T(8,128)(2,1)S(1)} %copy-done.5), kind=kOutput, calls=%fused_computation.2 | convolution fusion | flops 1613758464 | bytes 12320768 | tf_op jit(solution)/shard_map/rf,df->rd/dot_general | solution.py:84
  86.6 0.0 reduce-scatter.3.cloned.1.call-update
  86.6 0.0 reduce-scatter.5.cloned.1.call-start
  86.7 0.6 copy-done.12
  87.3 5.7 %all-gather.7.cloned.1.call-done = bf16[256,2048]{1,0:T(8,128)(2,1)} async-done(((bf16[256,512]{1,0:T(8,128)(2,1)}), bf16[256,2048]{1,0:T(8,128)(2,1)}) %all-gather.7.cloned.1.call-update) | async-done | bytes 1048592 | tf_op jit(solution)/shard_map/all_gather | solution.py:35
  93.0 0.0 copy-done.7
  93.0 2.4 %fusion.40 = (bf16[256,128]{1,0:T(8,128)(2,1)}, f32[256,128]{1,0:T(8,128)S(1)}) fusion(bf16[256,128]{1,0:T(8,128)(2,1)S(1)} %copy-done.7, bf16[256,128]{1,0:T(8,128)(2,1)S(1)} %copy-done.8, bf16[256,2048]{1,0:T(8,128)(2,1)} %all-gather.7.cloned.1.call-done, bf16[128,2048]{1,0:T(8,128)(2,1)S(1)} %copy-done.6), kind=kOutput, calls=%fused_computation.49 | convolution fusion | flops 134381568 | bytes 1900544 | tf_op jit(solution)/shard_map/td,cd->tc/dot_general | solution.py:100
  95.4 1.4 collective-permute-start
  96.8 1.4 convolution_bitcast_fusion
  98.2 0.0 reduce-scatter.5.cloned.1.call-update
  98.2 2.7 %collective-permute-done = f32[2,128]{1,0:T(2,128)S(1)} collective-permute-done((f32[2,128]{1,0:T(2,128)S(1)}, f32[2,128]{1,0:T(2,128)S(1)}, u32[]{:S(2)}, u32[]{:S(2)}) %collective-permute-start) | collective-permute-done | bytes 1056 | tf_op jit(solution)/shard_map/ppermute | solution.py:13
  101.0 0.7 multiply_convert_fusion.4
  101.6 0.7 multiply_convert_fusion.5
  102.3 30.8 %reduce-scatter.3.cloned.1.call-done = bf16[768,512]{1,0:T(8,128)(2,1)} async-done(((bf16[768,2048]{1,0:T(8,128)(2,1)}), bf16[768,512]{1,0:T(8,128)(2,1)}) %reduce-scatter.3.cloned.1.call-update) | async-done | bytes 786448 | tf_op jit(solution)/shard_map/reduce_scatter | solution.py:89
  133.1 5.5 %all-to-all-start.1 = ((bf16[8,96,512]{2,1,0:T(8,128)(2,1)}), bf16[8,96,512]{2,1,0:T(8,128)(2,1)S(1)}, u32[]{:S(2)}, u32[]{:S(2)}) async-start(bf16[8,96,512]{2,1,0:T(8,128)(2,1)} %bitcast.75), calls=%async_computation.2 | async-start | bytes 1572864 | tf_op jit(solution)/shard_map/all_to_all | solution.py:93
  138.6 5.3 %fusion.18 = bf16[1,2048,512]{1,2,0:T(8,128)(2,1)} fusion(bf16[768,512]{1,0:T(8,128)(2,1)} %copy-done.4, bf16[1,768,2048]{2,1,0:T(8,128)(2,1)} %all-gather.9.cloned.1.call-done), kind=kOutput, calls=%fused_computation.16 | convolution fusion | flops 1611661312 | bytes 6029312 | tf_op jit(solution)/shard_map/rd,rf->df/dot_general | solution.py:75
  143.9 3.9 %copy.27 = bf16[1,2048,512]{2,1,0:T(8,128)(2,1)} copy(bf16[1,2048,512]{1,2,0:T(8,128)(2,1)} %fusion.18) | data formatting | bytes 4194304
  147.8 5.3 %fusion.15 = bf16[1,2048,512]{1,2,0:T(8,128)(2,1)} fusion(bf16[768,512]{1,0:T(8,128)(2,1)} %copy-done.3, bf16[1,768,2048]{2,1,0:T(8,128)(2,1)} %all-gather.9.cloned.1.call-done), kind=kOutput, calls=%fused_computation.15 | convolution fusion | flops 1611661312 | bytes 6029312 | tf_op jit(solution)/shard_map/rd,rf->df/dot_general | solution.py:78
  153.1 3.9 %copy.28 = bf16[1,2048,512]{2,1,0:T(8,128)(2,1)} copy(bf16[1,2048,512]{1,2,0:T(8,128)(2,1)} %fusion.15) | data formatting | bytes 4194304
  157.0 6.2 %fusion.14 = bf16[1,512,2048]{2,1,0:T(8,128)(2,1)} fusion(bf16[768,2048]{1,0:T(8,128)(2,1)} %all-gather.5.cloned.1.call-done, f32[768,512]{1,0:T(8,128)} %fusion.6, f32[768,512]{1,0:T(8,128)} %fusion.4), kind=kOutput, calls=%fused_computation.14 | convolution fusion | flops 1615593472 | bytes 8388608 | tf_op jit(solution)/shard_map/rf,rd->fd/dot_general | solution.py:65
  163.2 1.4 all-to-all-done.1
  164.6 2.0 gather_fusion
  166.5 0.2 reshape.91
  166.7 2.1 reduce_sum.25
  168.8 36.7 %reduce-scatter.5.cloned.1.call-done = f32[256,128]{0,1:T(8,128)} async-done(((f32[2048,128]{0,1:T(8,128)}), f32[256,128]{0,1:T(8,128)}) %reduce-scatter.5.cloned.1.call-update) | async-done | bytes 131088 | tf_op jit(solution)/shard_map/reduce_scatter | solution.py:102
  (21 shorter events, 0.1 us)
Async XLA Ops:
  7.2 46.4 %copy-start = (bf16[1,2048,512]{2,1,0:T(8,128)(2,1)S(1)}, bf16[1,2048,512]{2,1,0:T(8,128)(2,1)}, u32[]{:S(2)}) copy-start(bf16[1,2048,512]{2,1,0:T(8,128)(2,1)} %param.17) | copy-start | bytes 6291460
  7.2 40.8 %all-gather.9.cloned.1.call-start = ((), (), s32[]{:S(2)}) async-start(), calls=%async_computation.8 | async-start | bytes 3932160 | tf_op jit(solution)/shard_map/all_gather | solution.py:53
  7.9 7.7 %copy-start.11 = (f32[256,2]{0,1:T(2,128)S(1)}, f32[256,2]{0,1:T(2,128)}, u32[]{:S(2)}) copy-start(f32[256,2]{0,1:T(2,128)} %param.15) | copy-start | bytes 6148
  7.9 66.7 %all-gather.5.cloned.1.call-start = ((), (), s32[]{:S(2)}) async-start(), calls=%async_computation.4 | async-start | bytes 3932160 | tf_op jit(solution)/shard_map/all_gather | solution.py:52
  47.0 46.0 %all-gather.7.cloned.1.call-start = ((), (), s32[]{:S(2)}) async-start(), calls=%async_computation.6 | async-start | bytes 1310720 | tf_op jit(solution)/shard_map/all_gather | solution.py:35
  47.7 85.4 %reduce-scatter.3.cloned.1.call-start = ((), (), s32[]{:S(2)}) async-start(), calls=%async_computation.5 | async-start | bytes 3932160 | tf_op jit(solution)/shard_map/reduce_scatter | solution.py:89
  47.9 5.6 %copy-start.1 = (bf16[1,768,2048]{2,1,0:T(8,128)(2,1)S(1)}, bf16[1,768,2048]{2,1,0:T(8,128)(2,1)}, u32[]{:S(2)}) copy-start(bf16[1,768,2048]{2,1,0:T(8,128)(2,1)} %all-gather.9.cloned.1.call-done) | copy-start | bytes 9437188
  80.8 1.9 copy-start.4
  80.8 1.9 copy-start.3
  80.8 2.2 %copy-start.5 = (bf16[1,2048,512]{2,1,0:T(8,128)(2,1)S(1)}, bf16[1,2048,512]{2,1,0:T(8,128)(2,1)}, u32[]{:S(2)}) copy-start(bf16[1,2048,512]{2,1,0:T(8,128)(2,1)} %param.18) | copy-start | bytes 6291460
  86.6 0.7 copy-start.12
  86.6 6.4 %copy-start.6 = (bf16[128,2048]{1,0:T(8,128)(2,1)S(1)}, bf16[128,2048]{1,0:T(8,128)(2,1)}, u32[]{:S(2)}) copy-start(bf16[128,2048]{1,0:T(8,128)(2,1)} %param.25) | copy-start | bytes 1572868
  86.6 6.4 %copy-start.7 = (bf16[256,128]{1,0:T(8,128)(2,1)S(1)}, bf16[256,128]{1,0:T(8,128)(2,1)}, u32[]{:S(2)}) copy-start(bf16[256,128]{1,0:T(8,128)(2,1)} %param.23) | copy-start | bytes 196612
  86.6 6.4 %copy-start.8 = (bf16[256,128]{1,0:T(8,128)(2,1)S(1)}, bf16[256,128]{1,0:T(8,128)(2,1)}, u32[]{:S(2)}) copy-start(bf16[256,128]{1,0:T(8,128)(2,1)} %param.22) | copy-start | bytes 196612
  86.6 118.9 %reduce-scatter.5.cloned.1.call-start = ((), (), s32[]{:S(2)}) async-start(), calls=%async_computation.7 | async-start | bytes 1179648 | tf_op jit(solution)/shard_map/reduce_scatter | solution.py:102
  93.0 3.8 %copy-start.2 = (bf16[256,2048]{1,0:T(8,128)(2,1)S(1)}, bf16[256,2048]{1,0:T(8,128)(2,1)}, u32[]{:S(2)}) copy-start(bf16[256,2048]{1,0:T(8,128)(2,1)} %all-gather.7.cloned.1.call-done) | copy-start | bytes 3145732
  95.4 5.6 %copy-start.9 = (bf16[256,128]{1,0:T(8,128)(2,1)S(1)}, bf16[256,128]{1,0:T(8,128)(2,1)}, u32[]{:S(2)}) copy-start(bf16[256,128]{1,0:T(8,128)(2,1)} %param.20) | copy-start | bytes 196612
  95.4 6.3 %copy-start.10 = (bf16[256,128]{1,0:T(8,128)(2,1)S(1)}, bf16[256,128]{1,0:T(8,128)(2,1)}, u32[]{:S(2)}) copy-start(bf16[256,128]{1,0:T(8,128)(2,1)} %param.21) | copy-start | bytes 196612
  95.4 5.6 %collective-permute-start = (f32[2,128]{1,0:T(2,128)S(1)}, f32[2,128]{1,0:T(2,128)S(1)}, u32[]{:S(2)}, u32[]{:S(2)}) collective-permute-start(f32[2,128]{1,0:T(2,128)S(1)} %slice.35), channel_id=1, source_target_pairs={{4,0},{8,4},{12,8},{16,12},{20,16},{24,20},{28,24},{5,1},{9,5},{13... | collective-permute-start | bytes 3080 | tf_op jit(solution)/shard_map/ppermute | solution.py:13
  133.1 31.5 %all-to-all-start.1 = ((bf16[8,96,512]{2,1,0:T(8,128)(2,1)}), bf16[8,96,512]{2,1,0:T(8,128)(2,1)S(1)}, u32[]{:S(2)}, u32[]{:S(2)}) async-start(bf16[8,96,512]{2,1,0:T(8,128)(2,1)} %bitcast.75), calls=%async_computation.2 | async-start | bytes 1572864 | tf_op jit(solution)/shard_map/all_to_all | solution.py:93
Sparse Core Ops, SparseCore 0:
  9.6 31.2 all-gather.8
  47.1 27.5 all-gather.4
  76.2 16.6 all-gather.6
  95.3 37.7 reduce-scatter.2
  136.9 68.5 reduce-scatter.4
where the time goes:
time: 213 us; the launch traced here: 212 us
  waiting for transfers between devices  96.8 us (45%)
  matrix products  40.6 us (19%)
  blocking collectives  27.5 us (13%)
  local copies, waits for them, and re-layouts  17 us (8%)
  between operations  14 us (7%)
  other arithmetic  8.79 us (4%)
  starting transfers between devices  7.3 us (3%)
    reduce_scatter x1, waiting for transfers between devices, per_device(): lax.psum_scatter(jnp.einsum('td,tc->dc', full_grad, mixed, preferred_elem...  36.7 us
    reduce_scatter x1, waiting for transfers between devices, per_device(): lax.psum_scatter(rounded_terms, 'tp', scatter_dimension=1, tiled=True)  30.8 us
    all_to_all x1, blocking collectives, per_device(): lax.all_to_all(buffer.reshape(sp_devices, capacity, -1), 'sp', split_axis...  27.5 us
    all_gather x1, waiting for transfers between devices, per_device(): lax.all_gather(arrived.reshape(sp_devices * capacity, -1), 'tp', axis=1,...  18.1 us
    unnamed x30, local copies, waits for them, and re-layouts  9.79 us
    dot_general x1, matrix products, per_device(): jnp.einsum('rf,rd->fd', hidden, expert_grad, preferred_element_type=jnp.f...  6.18 us
    dot_general x1, matrix products, per_device(): jnp.einsum('rd,fd->rf', expert_grad, down_weight, preferred_element_type=...  6.15 us
    all_gather x1, waiting for transfers between devices, per_device(): full_grad = lax.all_gather(layer_grad, 'tp', axis=1, tiled=True)  5.69 us
  transfers between devices with their start and end apart: 7, of which 6 were waited for; matrix products, arithmetic and copies ran while one was open for 31% of the time, Pallas kernels for 0%

commit v1 on v0

--- a/solution.py
+++ b/solution.py
@@ -49,7 +49,7 @@
         buffer.reshape(sp_devices, capacity, -1), "sp", split_axis=0, concat_axis=0, tiled=True
     )
     expert_grad, saved_rows = (
-        lax.all_gather(arrived.reshape(sp_devices * capacity, -1), "tp", axis=1, tiled=True),
+        jnp.concatenate(lax.all_gather(arrived.reshape(sp_devices * capacity, -1), "tp"), axis=1),
         lax.all_gather(expert_in[0], "tp", axis=1, tiled=True),
     )
     gate_weight = w_gate[0]

time: 213 us -> 213 us (level)
  waiting for transfers between devices: 96.8 us -> 91.8 us
  local copies, waits for them, and re-layouts: 17 us -> 21.6 us
    all_gather x1, waiting for transfers between devices: 5.69 us -> 0.98 us  [per_device(): full_grad = lax.all_gather(layer_grad, 'tp', axis=1, tiled=True)]
    all_gather x0 -> x1, local copies, waits for them, and re-layouts: none -> 4.66 us  [per_device(): lax.all_gather(arrived.reshape(sp_devices * capacity, -1), 'tp')]
  transfers between devices with their start and end apart: 7 -> 7, of which waited for: 6 -> 6; matrix products, arithmetic and copies ran while one was open for 31% -> 33% of each run, Pallas kernels for 0% -> 0%
where the time goes in v1:
time: 213 us; the launch traced here: 212 us
  waiting for transfers between devices  91.8 us (43%)
  matrix products  41 us (19%)
  blocking collectives  27.5 us (13%)
  local copies, waits for them, and re-layouts  21.6 us (10%)
  between operations  14 us (7%)
  other arithmetic  8.79 us (4%)
  starting transfers between devices  7.3 us (3%)
    reduce_scatter x1, waiting for transfers between devices, per_device(): lax.psum_scatter(jnp.einsum('td,tc->dc', full_grad, mixed, preferred_elem...  36.6 us
    reduce_scatter x1, waiting for transfers between devices, per_device(): lax.psum_scatter(rounded_terms, 'tp', scatter_dimension=1, tiled=True)  30.8 us
    all_to_all x1, blocking collectives, per_device(): lax.all_to_all(buffer.reshape(sp_devices, capacity, -1), 'sp', split_axis...  27.5 us
    all_gather x1, waiting for transfers between devices, per_device(): lax.all_gather(arrived.reshape(sp_devices * capacity, -1), 'tp')  18.1 us
    unnamed x30, local copies, waits for them, and re-layouts  9.74 us
    dot_general x1, matrix products, per_device(): jnp.einsum('rf,rd->fd', hidden, expert_grad, preferred_element_type=jnp.f...  6.41 us
    dot_general x1, matrix products, per_device(): jnp.einsum('rd,fd->rf', expert_grad, down_weight, preferred_element_type=...  6.25 us
    dot_general x1, matrix products, per_device(): up_pre = jnp.dot(saved_rows, up_weight, preferred_element_type=jnp.float32)  5.62 us
  transfers between devices with their start and end apart: 7, of which 6 were waited for; matrix products, arithmetic and copies ran while one was open for 33% of the time, Pallas kernels for 0%

profile of v1, /device:TPU:0, one launch (start us, length us, event | category | flops | bytes accessed | tf_op | source)
XLA Modules:
  0.0 212.0 jit_solution(17854373211226834599)
XLA Ops:
  7.2 0.0 copy-start
  7.2 0.0 all-gather.9.cloned.1.call-start
  7.2 0.7 all-gather.9.cloned.1.call-update
  7.9 0.0 copy-start.11
  7.9 0.0 all-gather.5.cloned.1.call-start
  8.0 0.8 copy.38
  8.8 0.1 eq.29
  8.9 0.1 eq.25
  9.1 0.7 broadcast_multiply_fusion
  9.8 0.1 copy.37
  9.9 0.1 mul.112
  10.1 1.1 reduce-window.6
  11.2 0.2 slice_reduce_fusion
  11.5 2.2 %mul.116 = f32[256,2,512]{2,1,0:T(2,128)} broadcast(bf16[256,512]{1,0:T(8,128)(2,1)} %param.13), dimensions={0,2} | broadcast | bytes 1310720 | tf_op jit(solution)/shard_map/mul | solution.py:43
  13.7 1.9 mul.117
  15.6 0.0 copy-done.11
  15.6 0.1 copy.40
  15.8 0.1 mul.114
  15.9 0.1 fusion.43
  16.0 3.4 %scatter_custom_fusion = bf16[768,512]{1,0:T(8,128)(2,1)} fusion(s32[512]{0:T(512)S(1)} %bitcast.81, f32[512,512]{1,0:T(8,128)S(1)} %mul.117, f32[512]{0:T(512)S(1)} %mul.114, bf16[]{:T(256)} %constant.11.clone.1), kind=kCustom, calls=%fused_computation.36 | custom fusion | flops 524288 | bytes 1837058 | tf_op jit(solution)/shard_map/scatter | solution.py:46
  19.4 27.5 %all_to_all.10 = bf16[8,96,512]{2,1,0:T(8,128)(2,1)} all-to-all(bf16[8,96,512]{2,1,0:T(8,128)(2,1)} %bitcast.76), channel_id=1, replica_groups=mesh['sp'=8,'tp'=4] {'sp'}, dimensions={0} | all-to-all | bytes 1572864 | tf_op jit(solution)/shard_map/all_to_all | solution.py:48
  46.9 0.0 all-gather.5.cloned.1.call-update
  47.0 0.0 all-gather.7.cloned.1.call-start
  47.0 0.7 all-gather.7.cloned.1.call-update
  47.7 0.2 reduce-scatter.3.cloned.1.call-start
  47.9 0.0 all-gather.9.cloned.1.call-done
  47.9 0.0 copy-start.1
  48.0 5.6 %fusion.4 = f32[768,512]{1,0:T(8,128)} fusion(bf16[1,768,2048]{2,1,0:T(8,128)(2,1)} %all-gather.9.cloned.1.call-done, bf16[1,2048,512]{2,1,0:T(8,128)(2,1)} %param.18), kind=kOutput, calls=%fused_computation.7 | convolution fusion | flops 1610612736 | bytes 6815744 | tf_op jit(solution)/shard_map/dot_general | solution.py:59
  53.6 0.0 copy-done
  53.6 0.0 copy-done.1
  53.6 3.0 %fusion.6 = f32[768,512]{1,0:T(8,128)} fusion(bf16[1,768,2048]{2,1,0:T(8,128)(2,1)S(1)} %copy-done.1, bf16[1,2048,512]{2,1,0:T(8,128)(2,1)S(1)} %copy-done), kind=kOutput, calls=%fused_computation.9 | convolution fusion | flops 1610612736 | bytes 6815744 | tf_op jit(solution)/shard_map/dot_general | solution.py:58
  56.6 18.1 %all-gather.5.cloned.1.call-done = bf16[4,768,512]{2,1,0:T(8,128)(2,1)} async-done(((bf16[1,768,512]{2,1,0:T(8,128)(2,1)}), bf16[4,768,512]{2,1,0:T(8,128)(2,1)}) %all-gather.5.cloned.1.call-update) | async-done | bytes 3145744 | tf_op jit(solution)/shard_map/all_gather | solution.py:52
  74.7 4.7 %copy.41 = bf16[4,768,512]{1,2,0:T(8,128)(2,1)} copy(bf16[4,768,512]{2,1,0:T(8,128)(2,1)} %all-gather.5.cloned.1.call-done) | data formatting | bytes 6291456 | tf_op jit(solution)/shard_map/all_gather | solution.py:52
  79.3 6.2 %select_convert_fusion = (bf16[768,512]{1,0:T(8,128)(2,1)S(1)}, bf16[768,512]{1,0:T(8,128)(2,1)S(1)}) fusion(f32[768,512]{1,0:T(8,128)} %fusion.4, f32[768,512]{1,0:T(8,128)} %fusion.6, bf16[768,2048]{0,1:T(8,128)(2,1)} %bitcast.77, bf16[1,512,2048]{2,1,0:T(8,128)(2,1)} %param.19), kind=kOutput, calls=%fused_computation.26 | convolution fusion | flops 1619263488 | bytes 9961472 | tf_op jit(solution)/shard_map/rd,fd->rf/dot_general | solution.py:64
  85.6 0.0 copy-start.4
  85.6 0.0 copy-start.5
  85.6 1.8 fusion.25
  87.5 0.3 copy-done.5
  87.8 3.5 %add_convert_fusion = bf16[768,2048]{1,0:T(8,128)(2,1)} fusion(f32[768,2048]{1,0:T(8,128)S(1)} %fusion.25, bf16[768,512]{1,0:T(8,128)(2,1)S(1)} %get-tuple-element.42, bf16[1,2048,512]{2,1,0:T(8,128)(2,1)S(1)} %copy-done.5), kind=kOutput, calls=%fused_computation.2 | convolution fusion | flops 1613758464 | bytes 12320768 | tf_op jit(solution)/shard_map/rf,df->rd/dot_general | solution.py:84
  91.3 0.0 reduce-scatter.3.cloned.1.call-update
  91.3 0.0 reduce-scatter.5.cloned.1.call-start
  91.4 0.6 copy-done.12
  92.0 1.0 all-gather.7.cloned.1.call-done
  93.0 2.4 %fusion.40 = (bf16[256,128]{1,0:T(8,128)(2,1)}, f32[256,128]{1,0:T(8,128)S(1)}) fusion(bf16[256,128]{1,0:T(8,128)(2,1)S(1)} %copy-done.7, bf16[256,128]{1,0:T(8,128)(2,1)S(1)} %copy-done.8, bf16[256,2048]{1,0:T(8,128)(2,1)} %all-gather.7.cloned.1.call-done, bf16[128,2048]{1,0:T(8,128)(2,1)S(1)} %copy-done.6), kind=kOutput, calls=%fused_computation.49 | convolution fusion | flops 134381568 | bytes 1900544 | tf_op jit(solution)/shard_map/td,cd->tc/dot_general | solution.py:100
  95.4 1.4 collective-permute-start
  96.8 0.0 copy-done.2
  96.8 1.4 convolution_bitcast_fusion
  98.2 0.0 reduce-scatter.5.cloned.1.call-update
  98.2 2.7 %collective-permute-done = f32[2,128]{1,0:T(2,128)S(1)} collective-permute-done((f32[2,128]{1,0:T(2,128)S(1)}, f32[2,128]{1,0:T(2,128)S(1)}, u32[]{:S(2)}, u32[]{:S(2)}) %collective-permute-start) | collective-permute-done | bytes 1056 | tf_op jit(solution)/shard_map/ppermute | solution.py:13
  101.0 0.0 copy-done.9
  101.0 0.7 multiply_convert_fusion.4
  101.6 0.7 multiply_convert_fusion.5
  102.3 30.8 %reduce-scatter.3.cloned.1.call-done = bf16[768,512]{1,0:T(8,128)(2,1)} async-done(((bf16[768,2048]{1,0:T(8,128)(2,1)}), bf16[768,512]{1,0:T(8,128)(2,1)}) %reduce-scatter.3.cloned.1.call-update) | async-done | bytes 786448 | tf_op jit(solution)/shard_map/reduce_scatter | solution.py:89
  133.1 5.5 %all-to-all-start.1 = ((bf16[8,96,512]{2,1,0:T(8,128)(2,1)}), bf16[8,96,512]{2,1,0:T(8,128)(2,1)S(1)}, u32[]{:S(2)}, u32[]{:S(2)}) async-start(bf16[8,96,512]{2,1,0:T(8,128)(2,1)} %bitcast.80), calls=%async_computation.2 | async-start | bytes 1572864 | tf_op jit(solution)/shard_map/all_to_all | solution.py:93
  138.6 5.3 %fusion.18 = bf16[1,2048,512]{1,2,0:T(8,128)(2,1)} fusion(bf16[768,512]{1,0:T(8,128)(2,1)} %copy-done.4, bf16[1,768,2048]{2,1,0:T(8,128)(2,1)} %all-gather.9.cloned.1.call-done), kind=kOutput, calls=%fused_computation.16 | convolution fusion | flops 1611661312 | bytes 6029312 | tf_op jit(solution)/shard_map/rd,rf->df/dot_general | solution.py:75
  143.9 3.9 %copy.42 = bf16[1,2048,512]{2,1,0:T(8,128)(2,1)} copy(bf16[1,2048,512]{1,2,0:T(8,128)(2,1)} %fusion.18) | data formatting | bytes 4194304
  147.8 5.3 %fusion.15 = bf16[1,2048,512]{1,2,0:T(8,128)(2,1)} fusion(bf16[768,512]{1,0:T(8,128)(2,1)} %copy-done.3, bf16[1,768,2048]{2,1,0:T(8,128)(2,1)} %all-gather.9.cloned.1.call-done), kind=kOutput, calls=%fused_computation.15 | convolution fusion | flops 1611661312 | bytes 6029312 | tf_op jit(solution)/shard_map/rd,rf->df/dot_general | solution.py:78
  153.1 3.9 %copy.43 = bf16[1,2048,512]{2,1,0:T(8,128)(2,1)} copy(bf16[1,2048,512]{1,2,0:T(8,128)(2,1)} %fusion.15) | data formatting | bytes 4194304
  157.0 6.4 %fusion.14 = bf16[1,512,2048]{2,1,0:T(8,128)(2,1)} fusion(bf16[768,2048]{0,1:T(8,128)(2,1)} %bitcast.78, f32[768,512]{1,0:T(8,128)} %fusion.6, f32[768,512]{1,0:T(8,128)} %fusion.4), kind=kOutput, calls=%fused_computation.14 | convolution fusion | flops 1615593472 | bytes 8388608 | tf_op jit(solution)/shard_map/rf,rd->fd/dot_general | solution.py:65
  163.4 1.1 all-to-all-done.1
  164.6 2.0 gather_fusion
  166.5 0.2 reshape.95
  166.7 2.1 reduce_sum.25
  168.8 36.6 %reduce-scatter.5.cloned.1.call-done = f32[256,128]{0,1:T(8,128)} async-done(((f32[2048,128]{0,1:T(8,128)}), f32[256,128]{0,1:T(8,128)}) %reduce-scatter.5.cloned.1.call-update) | async-done | bytes 131088 | tf_op jit(solution)/shard_map/reduce_scatter | solution.py:102
  (22 shorter events, 0.1 us)
Async XLA Ops:
  7.2 46.4 %copy-start = (bf16[1,2048,512]{2,1,0:T(8,128)(2,1)S(1)}, bf16[1,2048,512]{2,1,0:T(8,128)(2,1)}, u32[]{:S(2)}) copy-start(bf16[1,2048,512]{2,1,0:T(8,128)(2,1)} %param.17) | copy-start | bytes 6291460
  7.2 40.8 %all-gather.9.cloned.1.call-start = ((), (), s32[]{:S(2)}) async-start(), calls=%async_computation.8 | async-start | bytes 3932160 | tf_op jit(solution)/shard_map/all_gather | solution.py:53
  7.9 7.7 %copy-start.11 = (f32[256,2]{0,1:T(2,128)S(1)}, f32[256,2]{0,1:T(2,128)}, u32[]{:S(2)}) copy-start(f32[256,2]{0,1:T(2,128)} %param.15) | copy-start | bytes 6148
  7.9 66.7 %all-gather.5.cloned.1.call-start = ((), (), s32[]{:S(2)}) async-start(), calls=%async_computation.4 | async-start | bytes 3932160 | tf_op jit(solution)/shard_map/all_gather | solution.py:52
  47.0 46.0 %all-gather.7.cloned.1.call-start = ((), (), s32[]{:S(2)}) async-start(), calls=%async_computation.6 | async-start | bytes 1310720 | tf_op jit(solution)/shard_map/all_gather | solution.py:35
  47.7 85.4 %reduce-scatter.3.cloned.1.call-start = ((), (), s32[]{:S(2)}) async-start(), calls=%async_computation.5 | async-start | bytes 3932160 | tf_op jit(solution)/shard_map/reduce_scatter | solution.py:89
  47.9 5.6 %copy-start.1 = (bf16[1,768,2048]{2,1,0:T(8,128)(2,1)S(1)}, bf16[1,768,2048]{2,1,0:T(8,128)(2,1)}, u32[]{:S(2)}) copy-start(bf16[1,768,2048]{2,1,0:T(8,128)(2,1)} %all-gather.9.cloned.1.call-done) | copy-start | bytes 9437188
  85.6 1.9 copy-start.4
  85.6 1.9 copy-start.3
  85.6 2.2 %copy-start.5 = (bf16[1,2048,512]{2,1,0:T(8,128)(2,1)S(1)}, bf16[1,2048,512]{2,1,0:T(8,128)(2,1)}, u32[]{:S(2)}) copy-start(bf16[1,2048,512]{2,1,0:T(8,128)(2,1)} %param.18) | copy-start | bytes 6291460
  91.3 0.7 copy-start.12
  91.3 1.7 copy-start.6
  91.3 1.7 copy-start.7
  91.3 1.7 copy-start.8
  91.3 114.1 %reduce-scatter.5.cloned.1.call-start = ((), (), s32[]{:S(2)}) async-start(), calls=%async_computation.7 | async-start | bytes 1179648 | tf_op jit(solution)/shard_map/reduce_scatter | solution.py:102
  93.0 3.8 %copy-start.2 = (bf16[256,2048]{1,0:T(8,128)(2,1)S(1)}, bf16[256,2048]{1,0:T(8,128)(2,1)}, u32[]{:S(2)}) copy-start(bf16[256,2048]{1,0:T(8,128)(2,1)} %all-gather.7.cloned.1.call-done) | copy-start | bytes 3145732
  95.4 5.6 %copy-start.9 = (bf16[256,128]{1,0:T(8,128)(2,1)S(1)}, bf16[256,128]{1,0:T(8,128)(2,1)}, u32[]{:S(2)}) copy-start(bf16[256,128]{1,0:T(8,128)(2,1)} %param.20) | copy-start | bytes 196612
  95.4 6.3 %copy-start.10 = (bf16[256,128]{1,0:T(8,128)(2,1)S(1)}, bf16[256,128]{1,0:T(8,128)(2,1)}, u32[]{:S(2)}) copy-start(bf16[256,128]{1,0:T(8,128)(2,1)} %param.21) | copy-start | bytes 196612
  95.4 5.6 %collective-permute-start = (f32[2,128]{1,0:T(2,128)S(1)}, f32[2,128]{1,0:T(2,128)S(1)}, u32[]{:S(2)}, u32[]{:S(2)}) collective-permute-start(f32[2,128]{1,0:T(2,128)S(1)} %slice.35), channel_id=1, source_target_pairs={{4,0},{8,4},{12,8},{16,12},{20,16},{24,20},{28,24},{5,1},{9,5},{13... | collective-permute-start | bytes 3080 | tf_op jit(solution)/shard_map/ppermute | solution.py:13
  133.1 31.5 %all-to-all-start.1 = ((bf16[8,96,512]{2,1,0:T(8,128)(2,1)}), bf16[8,96,512]{2,1,0:T(8,128)(2,1)S(1)}, u32[]{:S(2)}, u32[]{:S(2)}) async-start(bf16[8,96,512]{2,1,0:T(8,128)(2,1)} %bitcast.80), calls=%async_computation.2 | async-start | bytes 1572864 | tf_op jit(solution)/shard_map/all_to_all | solution.py:93
Sparse Core Ops, SparseCore 0:
  9.6 31.2 all-gather.8
  47.1 27.5 all-gather.4
  76.2 16.6 all-gather.6
  95.3 37.7 reduce-scatter.2
  136.9 68.4 reduce-scatter.4
